TPU v7x, 32 devices: a whole 2x2x4 slice. The times are simulated.
32 devices in a mesh: sp: 8 (over z, y), tp: 4 (over x, core).
Axes of the slice: x: 2, y: 2, z: 4, core: 2. Of those that a mesh axis runs over, the one named last changes fastest.
Arguments:
- stream: bfloat16 [4096, 2048], P(('sp', 'tp')), may hold values from -6 to 6
- conv_value: bfloat16 [4096, 512], P('sp', 'tp'), may hold values from -6 to 6
- conv_gate: bfloat16 [4096, 512], P('sp', 'tp'), may hold values from -8 to 8
- doc_ids: int32 [4096], P('sp'), may hold values from 0 to 3, never falling along the last dimension, each value on 1 to 2048 neighbouring positions
- conv_taps: float32 [31, 512], P(None, 'tp'), may hold values from -2.2 to 2.2
- conv_bias: float32 [512], P('tp'), may hold values from -3 to 3
- chan_gain: float32 [512], replicated, may hold values from 0.1 to 1.9
- chan_shift: float32 [512], replicated, may hold values from -3 to 3
- out_weight: bfloat16 [512, 2048], replicated, may hold values from -0.25 to 0.25
- rms_gain: float32 [2048], replicated, may hold values from 0.1 to 1.9
- expert_ids: int32 [4096, 2], P(('sp', 'tp')), may hold values from 0 to 15, all different within a row; in each aligned block of 128 rows (0 to 127, 128 to 255, ...) at most 24 rows name the same one
- group_prob: float32 [4096], P(('sp', 'tp')), may hold values from 0.3 to 1
- route_logits: float32 [4096, 2], P(('sp', 'tp')), may hold values from -6 to 6
- expert_gate: bfloat16 [16, 2048, 1024], P('sp', None, 'tp'), may hold values from -0.125 to 0.125
- expert_up: bfloat16 [16, 2048, 1024], P('sp', None, 'tp'), may hold values from -0.125 to 0.125
- expert_down: bfloat16 [16, 1024, 2048], P('sp', 'tp'), may hold values from -0.1875 to 0.1875
Outputs:
- mixed: bfloat16 [4096, 2048], P(('sp', 'tp'))
Inputs may be any that keep to these rules, and one draw needn't show every extreme that they name: `expert_ids`: each row names 2 different experts. In each aligned block of 128 rows (the rows of one device) no expert is named by more than 24 rows, a bound that some block reaches. `doc_ids`: document numbers never fall along the sequence; every document has 1 to 2048 positions, one exactly 2048.
All inputs are finite; a program needn't handle non-finite values.
Results may differ from a plain program's by a relative error of at most 0.012.
Values may be sent and summed in bfloat16 or wider, within the bound.
A program may use at most 64 MiB of HBM per device.

v0:
```python
import jax
import jax.numpy as jnp
from jax import lax
from jax.sharding import PartitionSpec as P

CONV_CH = 512
eps = 1e-06


def passed_along(x, axis, by):
    size = lax.axis_size(axis)
    pairs = [(i, i + by) for i in range(size) if 0 <= i + by < size]
    return lax.ppermute(x, axis, pairs)


def causal_conv(values, gates, docs, conv_taps, conv_bias):
    reach = conv_taps.shape[0] - 1
    acts = values.astype(jnp.float32) * jax.nn.sigmoid(gates.astype(jnp.float32))
    total = values.shape[0] - reach
    result = jnp.broadcast_to(conv_bias[None, :], (total, values.shape[1]))
    own_doc = docs[reach:]
    for offset in range(reach + 1):
        begin = reach - offset
        same = (docs[begin : begin + total] == own_doc)[:, None]
        result = (
            result + jnp.where(same, acts[begin : begin + total], 0.0) * conv_taps[offset][None, :]
        )
    return result.astype(jnp.bfloat16)


def finish_norm(values, mean, square, gain, shift):
    spread = square - mean * mean
    scaled = (values - mean) * lax.rsqrt(spread + eps) * gain + shift
    return jax.nn.silu(scaled).astype(jnp.bfloat16)


def apply_experts(arrived, expert_gate, expert_up, expert_down):
    outputs = []
    for local in range(arrived.shape[1]):
        rows = arrived[:, local].reshape(-1, arrived.shape[3])
        gated = jnp.dot(rows, expert_gate[local], preferred_element_type=jnp.float32)
        upward = jnp.dot(rows, expert_up[local], preferred_element_type=jnp.float32)
        hidden = (jax.nn.silu(gated) * upward).astype(jnp.bfloat16)
        partial_value = jnp.dot(hidden, expert_down[local], preferred_element_type=jnp.float32)
        outputs.append(partial_value.reshape(arrived.shape[0], arrived.shape[2], arrived.shape[3]))
    return jnp.stack(outputs, axis=1)


def split_quarters(partial_value, quarters):
    shape = partial_value.shape
    return partial_value.astype(jnp.bfloat16).reshape(
        shape[0], shape[1], quarters, shape[2] // quarters, shape[3]
    )


def body(
    stream,
    conv_value,
    conv_gate,
    doc_ids,
    conv_taps,
    conv_bias,
    chan_gain,
    chan_shift,
    out_weight,
    rms_gain,
    expert_ids,
    group_prob,
    route_logits,
    expert_gate,
    expert_up,
    expert_down,
):
    reach = conv_taps.shape[0] - 1
    tail_value, tail_gate, tail_doc = passed_along(
        (conv_value[-reach:], conv_gate[-reach:], doc_ids[-reach:]), "sp", 1
    )
    values = jnp.concatenate([tail_value, conv_value], axis=0)
    gates = jnp.concatenate([tail_gate, conv_gate], axis=0)
    docs = jnp.concatenate([tail_doc, doc_ids], axis=0)
    conved = causal_conv(values, gates, docs, conv_taps, conv_bias)
    own_rows = stream.shape[0]
    width_local = conved.shape[1]
    lane = lax.axis_index("tp") * width_local
    floats = conved.astype(jnp.float32)
    sums, squares = lax.psum((jnp.sum(floats, axis=1), jnp.sum(floats * floats, axis=1)), "tp")
    mean = (sums / CONV_CH)[:, None]
    square = (squares / CONV_CH)[:, None]
    gain = lax.dynamic_slice_in_dim(chan_gain, lane, width_local, 0)
    shift = lax.dynamic_slice_in_dim(chan_shift, lane, width_local, 0)
    activated = finish_norm(floats, mean, square, gain, shift)
    weight_rows = lax.dynamic_slice_in_dim(out_weight, lane, width_local, 0)
    projected = lax.psum_scatter(
        jnp.dot(activated, weight_rows, preferred_element_type=jnp.float32).astype(jnp.bfloat16),
        "tp",
        scatter_dimension=0,
        tiled=True,
    ).astype(jnp.float32)
    resid = (stream.astype(jnp.float32) + projected).astype(jnp.bfloat16)
    resid_float = resid.astype(jnp.float32)
    mean_square = jnp.mean(resid_float * resid_float, axis=-1, keepdims=True)
    normed = (resid_float * lax.rsqrt(mean_square + eps) * rms_gain).astype(jnp.bfloat16)
    gap = route_logits[:, 0] - route_logits[:, 1]
    weights = jnp.stack(
        [group_prob * jax.nn.sigmoid(gap), group_prob * jax.nn.sigmoid(-gap)], axis=1
    )
    sp_count = lax.axis_size("sp")
    tp_count = lax.axis_size("tp")
    local_experts = expert_gate.shape[0]
    experts_all = sp_count * local_experts
    top_count = expert_ids.shape[1]
    capacity = max(2, 3 * own_rows * top_count // (2 * experts_all))
    flat_ids = expert_ids.reshape(-1)
    onehot = (flat_ids[:, None] == jnp.arange(experts_all, dtype=jnp.int32)[None, :]).astype(
        jnp.int32
    )
    earlier = jnp.cumsum(onehot, axis=0) - onehot
    ranks = jnp.sum(earlier * onehot, axis=1)
    dest = flat_ids * capacity + ranks
    route_token = jnp.arange(flat_ids.shape[0], dtype=jnp.int32) // top_count
    source = jnp.full((experts_all * capacity,), own_rows, jnp.int32).at[dest].set(route_token)
    with_blank = jnp.concatenate([normed, jnp.zeros((1, normed.shape[1]), jnp.bfloat16)], axis=0)
    outgoing = with_blank[source].reshape(sp_count, local_experts, capacity, normed.shape[1])
    arrived_own = lax.all_to_all(outgoing, "sp", split_axis=0, concat_axis=0, tiled=True)
    arrived = lax.all_gather(arrived_own, "tp", axis=2, tiled=True)
    partial_value = apply_experts(arrived, expert_gate, expert_up, expert_down)
    quarters = lax.all_to_all(
        split_quarters(partial_value, tp_count), "tp", split_axis=2, concat_axis=2, tiled=True
    )
    summed = jnp.sum(quarters.astype(jnp.float32), axis=2).astype(jnp.bfloat16)
    routed = lax.all_to_all(summed, "sp", split_axis=0, concat_axis=0, tiled=True)
    flat_out = routed.reshape(experts_all * capacity, normed.shape[1])
    picked = flat_out[dest].reshape(own_rows, top_count, normed.shape[1]).astype(jnp.float32)
    combined = jnp.sum(weights[:, :, None] * picked, axis=1)
    return (resid_float + combined).astype(jnp.bfloat16)


def solution(mesh):
    placed = (
        P(("sp", "tp"), None),
        P("sp", "tp"),
        P("sp", "tp"),
        P("sp"),
        P(None, "tp"),
        P("tp"),
        P(),
        P(),
        P(),
        P(),
        P(("sp", "tp"), None),
        P(("sp", "tp")),
        P(("sp", "tp"), None),
        P("sp", None, "tp"),
        P("sp", None, "tp"),
        P("sp", "tp", None),
    )
    return jax.shard_map(
        body, mesh=mesh, in_specs=placed, out_specs=P(("sp", "tp"), None), check_vma=False
    )
```

profile of v0, /device:TPU:0, one launch (start us, length us, event | category | flops | bytes accessed | tf_op | source)
XLA Modules:
  0.0 321.5 jit_solution(74922192068838987)
XLA Ops:
  6.5 0.0 reduce-scatter.2.cloned.1.call-start
  6.5 0.9 slice.325
  7.4 4.9 %collective-permute-start.2 = (s32[30]{0:T(128)S(1)}, s32[30]{0:T(128)S(1)}, u32[]{:S(2)}, u32[]{:S(2)}) collective-permute-start(s32[30]{0:T(128)S(1)} %slice.325), channel_id=1, source_target_pairs={{0,4},{4,8},{8,12},{12,16},{16,20},{20,24},{24,28},{1,5},{5,9},{9,... | collective-permute-start | bytes 368 | tf_op jit(solution)/shard_map/ppermute | solution.py:13
  12.3 0.7 slice.321
  13.0 3.4 %collective-permute-start = (bf16[30,128]{1,0:T(8,128)(2,1)S(1)}, bf16[30,128]{1,0:T(8,128)(2,1)S(1)}, u32[]{:S(2)}, u32[]{:S(2)}) collective-permute-start(bf16[30,128]{1,0:T(8,128)(2,1)S(1)} %slice.321), channel_id=1, source_target_pairs={{0,4},{4,8},{8,12},{12,16},{16,20},{20,24},{24,28},{1,5},{5,9},{9,... | collective-permute-start | bytes 23048 | tf_op jit(solution)/shard_map/ppermute | solution.py:13
  16.5 0.7 slice.322
  17.2 3.4 %collective-permute-start.1 = (bf16[30,128]{1,0:T(8,128)(2,1)S(1)}, bf16[30,128]{1,0:T(8,128)(2,1)S(1)}, u32[]{:S(2)}, u32[]{:S(2)}) collective-permute-start(bf16[30,128]{1,0:T(8,128)(2,1)S(1)} %slice.322), channel_id=1, source_target_pairs={{0,4},{4,8},{8,12},{12,16},{16,20},{20,24},{24,28},{1,5},{5,9},{9,... | collective-permute-start | bytes 23048 | tf_op jit(solution)/shard_map/ppermute | solution.py:13
  20.6 1.0 slice_bitcast_fusion.30
  21.6 1.0 slice_bitcast_fusion.29
  22.6 0.8 dynamic_slice.10
  23.3 0.8 dynamic_slice.9
  24.1 0.0 collective-permute-done.2
  24.1 0.8 pad_add_fusion
  24.8 0.8 slice_compare_fusion.29
  25.6 0.8 slice_compare_fusion.28
  26.4 0.0 collective-permute-done
  26.4 0.0 collective-permute-done.1
  26.4 1.1 divide_multiply_fusion
  27.5 3.8 %convert_reduce_fusion = (f32[512]{0:T(512)S(1)}, f32[512]{0:T(512)S(1)}, bf16[512,128]{1,0:T(8,128)(2,1)S(1)}) fusion(f32[128]{0:T(128)S(1)} %get-tuple-element.41, f32[542,128]{1,0:T(8,128)S(1)} %divide_multiply_fusion, pred[512]{0:T(512)(128)(4,1)S(1)} %get-tuple-element.71, f32[128]{0:T(128)S(1)} %get-tuple-element.42, ...), kind=kLoop, calls=%fused_computation.39 | loop fusion | flops 6355968 | bytes 8293376 | tf_op jit(solution)/shard_map/reduce_sum | solution.py:86
  31.3 0.0 copy-start.4
  31.4 0.0 copy-start.1
  31.4 5.9 %all-reduce.1 = (f32[512]{0:T(512)S(1)}, f32[512]{0:T(512)S(1)}) all-reduce(f32[512]{0:T(512)S(1)} %get-tuple-element.6, f32[512]{0:T(512)S(1)} %get-tuple-element.5), channel_id=1, replica_groups=mesh['sp'=8,'tp'=4] {'tp'}, use_global_device_ids=true, to_apply=%region_3.4 | all-reduce | flops 1024 | bytes 8192 | tf_op jit(solution)/shard_map/psum | solution.py:86
  37.3 2.1 convolution_convert_fusion.2
  39.4 0.0 reduce-scatter.2.cloned.1.call-update
  39.4 0.0 all-gather.2.cloned.1.call-start
  39.5 0.1 copy.33
  39.6 0.1 eq.149
  39.8 0.1 eq.145
  39.9 0.6 reduce-window.6
  40.5 0.2 slice_reduce_fusion
  40.7 0.1 copy.32
  40.8 0.1 mul.520
  41.0 0.1 fusion.103
  41.1 1.4 scatter_custom_fusion
  42.5 27.7 %reduce-scatter.2.cloned.1.call-done = bf16[128,2048]{1,0:T(8,128)(2,1)} async-done(((bf16[512,2048]{1,0:T(8,128)(2,1)}), bf16[128,2048]{1,0:T(8,128)(2,1)}) %reduce-scatter.2.cloned.1.call-update) | async-done | bytes 524304 | tf_op jit(solution)/shard_map/reduce_scatter | solution.py:93
  70.2 1.3 fusion.4
  71.5 1.3 fusion.6
  72.8 3.1 gather_fusion
  76.0 42.4 %all_to_all.15 = bf16[8,2,24,2048]{3,2,1,0:T(8,128)(2,1)} all-to-all(bf16[8,2,24,2048]{3,2,1,0:T(8,128)(2,1)} %bitcast.137), channel_id=1, replica_groups=mesh['sp'=8,'tp'=4] {'sp'}, dimensions={0} | all-to-all | bytes 3145728 | tf_op jit(solution)/shard_map/all_to_all | solution.py:124
  118.4 0.0 all-gather.2.cloned.1.call-update
  118.4 44.6 %all-gather.2.cloned.1.call-done = bf16[8,2,96,2048]{3,2,1,0:T(8,128)(2,1)} async-done(((bf16[8,2,24,2048]{3,2,1,0:T(8,128)(2,1)}), bf16[8,2,96,2048]{3,2,1,0:T(8,128)(2,1)}) %all-gather.2.cloned.1.call-update) | async-done | bytes 6291472 | tf_op jit(solution)/shard_map/all_gather | solution.py:125
  163.0 3.6 %fusion.112 = (bf16[8,1,96,2048]{3,2,1,0:T(8,128)(2,1)S(1)}, bf16[8,1,96,2048]{3,2,1,0:T(8,128)(2,1)S(1)}) fusion(bf16[8,2,96,2048]{3,2,1,0:T(8,128)(2,1)} %all-gather.2.cloned.1.call-done), kind=kLoop, calls=%fused_computation.242 | loop fusion | bytes 12582912 | tf_op jit(solution)/shard_map/slice | solution.py:40
  166.6 1.0 fusion.14
  167.6 0.0 copy-start.8
  167.6 1.0 fusion.11
  168.6 0.6 copy-done.8
  169.2 1.0 fusion.2
  170.2 0.0 copy-start.9
  170.2 1.0 fusion.3
  171.2 0.6 copy-done.9
  171.8 1.0 fusion
  172.8 1.0 fusion.1
  173.8 0.6 pad_maximum_fusion
  174.4 1.1 copy.36
  175.5 74.2 %all_to_all.16 = bf16[8,2,4,24,2048]{4,3,0,1,2:T(8,128)(2,1)} all-to-all(bf16[8,2,4,24,2048]{4,3,0,1,2:T(8,128)(2,1)S(1)} %copy.36), channel_id=1, replica_groups=mesh['sp'=8,'tp'=4] {'tp'}, dimensions={2} | all-to-all | bytes 12582912 | tf_op jit(solution)/shard_map/all_to_all | solution.py:127
  249.7 5.7 %reduce_sum.64 = bf16[8,2,24,2048]{3,2,0,1:T(8,128)(2,1)} reduce(bf16[8,2,4,24,2048]{4,3,0,1,2:T(8,128)(2,1)} %all_to_all.16, bf16[]{:T(256)} %constant.56.clone.1), dimensions={2}, to_apply=%region_10.11 | reduce | flops 2359296 | bytes 7864322 | tf_op jit(solution)/shard_map/reduce_sum | solution.py:130
  255.4 2.8 copy.38
  258.1 5.5 %all-to-all-start.2 = ((bf16[8,2,24,2048]{3,2,1,0:T(8,128)(2,1)}), bf16[8,2,24,2048]{3,2,1,0:T(8,128)(2,1)}, u32[]{:S(2)}, u32[]{:S(2)}) async-start(bf16[8,2,24,2048]{3,2,1,0:T(8,128)(2,1)} %copy.38), calls=%async_computation.3 | async-start | bytes 3145728 | tf_op jit(solution)/shard_map/all_to_all | solution.py:131
  263.7 0.1 copy.31
  263.8 36.6 %all-to-all-done.2 = bf16[8,2,24,2048]{3,2,1,0:T(8,128)(2,1)} async-done(((bf16[8,2,24,2048]{3,2,1,0:T(8,128)(2,1)}), bf16[8,2,24,2048]{3,2,1,0:T(8,128)(2,1)}, u32[]{:S(2)}, u32[]{:S(2)}) %all-to-all-start.2) | async-done | bytes 1572896 | tf_op jit(solution)/shard_map/all_to_all | solution.py:131
  300.4 5.0 %gather_fusion.1 = bf16[256,2048]{1,0:T(8,128)(2,1)} fusion(bf16[384,2048]{1,0:T(8,128)(2,1)} %bitcast.55, s32[1024]{0:T(1024)S(1)} %pad_clamp_fusion), kind=kCustom, calls=%fused_computation.1 | custom fusion | bytes 2098176 | tf_op jit(solution)/shard_map/gather | solution.py:133
  305.4 3.5 %reshape.150 = f32[128,2,2048]{2,1,0:T(2,128)} reshape(bf16[256,2048]{1,0:T(8,128)(2,1)} %gather_fusion.1) | data formatting | bytes 3145728 | tf_op jit(solution)/shard_map/convert_element_type | solution.py:133
  308.8 4.8 %multiply_reduce_fusion = f32[128,2048]{1,0:T(8,128)S(1)} fusion(f32[128,2,2048]{2,1,0:T(2,128)} %reshape.150, f32[128,2]{1,0:T(8,128)S(1)} %copy.31), kind=kLoop, calls=%fused_computation.9 | loop fusion | flops 786432 | bytes 3146752 | tf_op jit(solution)/shard_map/reduce_sum | solution.py:134
  313.6 1.0 fusion.7
  (28 shorter events, 0.2 us)
Async XLA Ops:
  6.5 30.7 %copy-start = (bf16[512,2048]{1,0:T(8,128)(2,1)S(1)}, bf16[512,2048]{1,0:T(8,128)(2,1)}, u32[]{:S(2)}) copy-start(bf16[512,2048]{1,0:T(8,128)(2,1)} %param.24) | copy-start | bytes 6291460
  6.5 63.7 %reduce-scatter.2.cloned.1.call-start = ((), (), s32[]{:S(2)}) async-start(), calls=%async_computation.4 | async-start | bytes 2621440 | tf_op jit(solution)/shard_map/reduce_scatter | solution.py:93
  7.4 16.6 %collective-permute-start.2 = (s32[30]{0:T(128)S(1)}, s32[30]{0:T(128)S(1)}, u32[]{:S(2)}, u32[]{:S(2)}) collective-permute-start(s32[30]{0:T(128)S(1)} %slice.325), channel_id=1, source_target_pairs={{0,4},{4,8},{8,12},{12,16},{16,20},{20,24},{24,28},{1,5},{5,9},{9,... | collective-permute-start | bytes 368 | tf_op jit(solution)/shard_map/ppermute | solution.py:13
  13.0 13.4 %collective-permute-start = (bf16[30,128]{1,0:T(8,128)(2,1)S(1)}, bf16[30,128]{1,0:T(8,128)(2,1)S(1)}, u32[]{:S(2)}, u32[]{:S(2)}) collective-permute-start(bf16[30,128]{1,0:T(8,128)(2,1)S(1)} %slice.321), channel_id=1, source_target_pairs={{0,4},{4,8},{8,12},{12,16},{16,20},{20,24},{24,28},{1,5},{5,9},{9,... | collective-permute-start | bytes 23048 | tf_op jit(solution)/shard_map/ppermute | solution.py:13
  17.2 9.2 %collective-permute-start.1 = (bf16[30,128]{1,0:T(8,128)(2,1)S(1)}, bf16[30,128]{1,0:T(8,128)(2,1)S(1)}, u32[]{:S(2)}, u32[]{:S(2)}) collective-permute-start(bf16[30,128]{1,0:T(8,128)(2,1)S(1)} %slice.322), channel_id=1, source_target_pairs={{0,4},{4,8},{8,12},{12,16},{16,20},{20,24},{24,28},{1,5},{5,9},{9,... | collective-permute-start | bytes 23048 | tf_op jit(solution)/shard_map/ppermute | solution.py:13
  31.3 8.1 %copy-start.4 = (s32[128,2]{0,1:T(2,128)S(1)}, s32[128,2]{0,1:T(2,128)}, u32[]{:S(2)}) copy-start(s32[128,2]{0,1:T(2,128)} %param.26) | copy-start | bytes 3076
  31.4 38.9 %copy-start.1 = (bf16[128,2048]{1,0:T(8,128)(2,1)S(1)}, bf16[128,2048]{1,0:T(8,128)(2,1)}, u32[]{:S(2)}) copy-start(bf16[128,2048]{1,0:T(8,128)(2,1)} %param.16) | copy-start | bytes 1572868
  37.3 34.3 %copy-start.3 = (f32[2048]{0:T(1024)S(1)}, f32[2048]{0:T(1024)}, u32[]{:S(2)}) copy-start(f32[2048]{0:T(1024)} %param.25) | copy-start | bytes 24580
  39.4 123.6 %all-gather.2.cloned.1.call-start = ((), (), s32[]{:S(2)}) async-start(), calls=%async_computation.5 | async-start | bytes 7864320 | tf_op jit(solution)/shard_map/all_gather | solution.py:125
  163.0 3.6 %copy-start.7 = (bf16[2,2048,256]{2,1,0:T(8,128)(2,1)S(1)}, bf16[2,2048,256]{2,1,0:T(8,128)(2,1)}, u32[]{:S(2)}) copy-start(bf16[2,2048,256]{2,1,0:T(8,128)(2,1)} %param.29) | copy-start | bytes 6291460
  167.6 1.6 copy-start.8
  170.2 1.6 copy-start.9
  255.4 8.3 %copy-start.5 = (f32[128,2]{0,1:T(2,128)S(1)}, f32[128,2]{0,1:T(2,128)}, u32[]{:S(2)}) copy-start(f32[128,2]{0,1:T(2,128)} %param.28) | copy-start | bytes 3076
  255.4 8.3 %copy-start.6 = (f32[128]{0:T(128)S(1)}, f32[128]{0:T(128)}, u32[]{:S(2)}) copy-start(f32[128]{0:T(128)} %param.27) | copy-start | bytes 1540
  258.1 42.3 %all-to-all-start.2 = ((bf16[8,2,24,2048]{3,2,1,0:T(8,128)(2,1)}), bf16[8,2,24,2048]{3,2,1,0:T(8,128)(2,1)}, u32[]{:S(2)}, u32[]{:S(2)}) async-start(bf16[8,2,24,2048]{3,2,1,0:T(8,128)(2,1)} %copy.38), calls=%async_computation.3 | async-start | bytes 3145728 | tf_op jit(solution)/shard_map/all_to_all | solution.py:131
  305.4 8.3 %copy-start.2 = (bf16[128,2048]{1,0:T(8,128)(2,1)S(1)}, bf16[128,2048]{1,0:T(8,128)(2,1)}, u32[]{:S(2)}) copy-start(bf16[128,2048]{1,0:T(8,128)(2,1)} %reduce-scatter.2.cloned.1.call-done) | copy-start | bytes 1572868
Sparse Core Ops, SparseCore 0:
  39.6 30.6 reduce-scatter.1
  118.6 44.4 all-gather.1
where the time goes:
time: 322 us; the launch traced here: 321 us
  blocking collectives  123 us (38%)
  waiting for transfers between devices  109 us (34%)
  local copies, waits for them, and re-layouts  28.4 us (9%)
  other arithmetic  22.6 us (7%)
  starting transfers between devices  17.3 us (5%)
  between operations  13.7 us (4%)
  matrix products  8.06 us (3%)
    all_to_all x1, blocking collectives, body(): lax.all_to_all(split_quarters(partial_value, tp_count), 'tp', split_axis=...  74.2 us
    all_gather x1, waiting for transfers between devices, body(): arrived = lax.all_gather(arrived_own, 'tp', axis=2, tiled=True)  44.6 us
    all_to_all x1, blocking collectives, body(): lax.all_to_all(outgoing, 'sp', split_axis=0, concat_axis=0, tiled=True)  42.4 us
    all_to_all x1, waiting for transfers between devices, body(): lax.all_to_all(summed, 'sp', split_axis=0, concat_axis=0, tiled=True)  36.6 us
    reduce_scatter x1, waiting for transfers between devices, body(): lax.psum_scatter(jnp.dot(activated, weight_rows, preferred_element_type=j...  27.7 us
    ppermute x3, starting transfers between devices, passed_along(): return lax.ppermute(x, axis, pairs)  11.7 us
  transfers between devices with their start and end apart: 6, of which 3 were waited for; matrix products, arithmetic and copies ran while one was open for 3% of the time, Pallas kernels for 0%

commit v1 on v0

--- a/solution.py
+++ b/solution.py
@@ -124,8 +124,16 @@
     arrived_own = lax.all_to_all(outgoing, "sp", split_axis=0, concat_axis=0, tiled=True)
     arrived = lax.all_gather(arrived_own, "tp", axis=2, tiled=True)
     partial_value = apply_experts(arrived, expert_gate, expert_up, expert_down)
-    quarters = lax.all_to_all(
-        split_quarters(partial_value, tp_count), "tp", split_axis=2, concat_axis=2, tiled=True
+    quarters = jnp.concatenate(
+        lax.all_to_all(
+            jnp.stack(
+                jnp.split(split_quarters(partial_value, tp_count), lax.axis_size("tp"), axis=2)
+            ),
+            "tp",
+            0,
+            0,
+        ),
+        axis=2,
     )
     summed = jnp.sum(quarters.astype(jnp.float32), axis=2).astype(jnp.bfloat16)
     routed = lax.all_to_all(summed, "sp", split_axis=0, concat_axis=0, tiled=True)

time: 322 us -> 322 us (level)
  no operation moved by 1% of the time
where the time goes in v1:
time: 322 us; the launch traced here: 321 us
  blocking collectives  122 us (38%)
  waiting for transfers between devices  109 us (34%)
  local copies, waits for them, and re-layouts  27.2 us (8%)
  other arithmetic  23.5 us (7%)
  starting transfers between devices  17.4 us (5%)
  between operations  13.7 us (4%)
  matrix products  8.07 us (3%)
    all_to_all x1, blocking collectives, body(): lax.all_to_all(jnp.stack(jnp.split(split_quarters(partial_value, tp_count...  74.2 us
    all_gather x1, waiting for transfers between devices, body(): arrived = lax.all_gather(arrived_own, 'tp', axis=2, tiled=True)  44.6 us
    all_to_all x1, blocking collectives, body(): lax.all_to_all(outgoing, 'sp', split_axis=0, concat_axis=0, tiled=True)  42.5 us
    all_to_all x1, waiting for transfers between devices, body(): lax.all_to_all(summed, 'sp', split_axis=0, concat_axis=0, tiled=True)  36.6 us
    reduce_scatter x1, waiting for transfers between devices, body(): lax.psum_scatter(jnp.dot(activated, weight_rows, preferred_element_type=j...  27.6 us
    ppermute x3, starting transfers between devices, passed_along(): return lax.ppermute(x, axis, pairs)  11.7 us
  transfers between devices with their start and end apart: 6, of which 3 were waited for; matrix products, arithmetic and copies ran while one was open for 3% of the time, Pallas kernels for 0%

profile of v1, /device:TPU:0, one launch (start us, length us, event | category | flops | bytes accessed | tf_op | source)
XLA Modules:
  0.0 321.2 jit_solution(3979163487419886621)
XLA Ops:
  6.5 0.0 reduce-scatter.2.cloned.1.call-start
  6.5 0.9 slice.325
  7.4 4.9 %collective-permute-start.2 = (s32[30]{0:T(128)S(1)}, s32[30]{0:T(128)S(1)}, u32[]{:S(2)}, u32[]{:S(2)}) collective-permute-start(s32[30]{0:T(128)S(1)} %slice.325), channel_id=1, source_target_pairs={{0,4},{4,8},{8,12},{12,16},{16,20},{20,24},{24,28},{1,5},{5,9},{9,... | collective-permute-start | bytes 368 | tf_op jit(solution)/shard_map/ppermute | solution.py:13
  12.3 0.7 slice.321
  13.0 3.4 %collective-permute-start = (bf16[30,128]{1,0:T(8,128)(2,1)S(1)}, bf16[30,128]{1,0:T(8,128)(2,1)S(1)}, u32[]{:S(2)}, u32[]{:S(2)}) collective-permute-start(bf16[30,128]{1,0:T(8,128)(2,1)S(1)} %slice.321), channel_id=1, source_target_pairs={{0,4},{4,8},{8,12},{12,16},{16,20},{20,24},{24,28},{1,5},{5,9},{9,... | collective-permute-start | bytes 23048 | tf_op jit(solution)/shard_map/ppermute | solution.py:13
  16.5 0.7 slice.322
  17.2 3.4 %collective-permute-start.1 = (bf16[30,128]{1,0:T(8,128)(2,1)S(1)}, bf16[30,128]{1,0:T(8,128)(2,1)S(1)}, u32[]{:S(2)}, u32[]{:S(2)}) collective-permute-start(bf16[30,128]{1,0:T(8,128)(2,1)S(1)} %slice.322), channel_id=1, source_target_pairs={{0,4},{4,8},{8,12},{12,16},{16,20},{20,24},{24,28},{1,5},{5,9},{9,... | collective-permute-start | bytes 23048 | tf_op jit(solution)/shard_map/ppermute | solution.py:13
  20.6 1.0 slice_bitcast_fusion.30
  21.6 1.0 slice_bitcast_fusion.29
  22.6 0.8 dynamic_slice.10
  23.3 0.8 dynamic_slice.9
  24.1 0.0 collective-permute-done.2
  24.1 0.8 pad_add_fusion
  24.8 0.8 slice_compare_fusion.29
  25.6 0.8 slice_compare_fusion.28
  26.4 0.0 collective-permute-done
  26.4 0.0 collective-permute-done.1
  26.4 1.1 divide_multiply_fusion
  27.5 3.8 %convert_reduce_fusion = (f32[512]{0:T(512)S(1)}, f32[512]{0:T(512)S(1)}, bf16[512,128]{1,0:T(8,128)(2,1)S(1)}) fusion(f32[128]{0:T(128)S(1)} %get-tuple-element.45, f32[542,128]{1,0:T(8,128)S(1)} %divide_multiply_fusion, pred[512]{0:T(512)(128)(4,1)S(1)} %get-tuple-element.75, f32[128]{0:T(128)S(1)} %get-tuple-element.46, ...), kind=kLoop, calls=%fused_computation.53 | loop fusion | flops 6355968 | bytes 8293376 | tf_op jit(solution)/shard_map/reduce_sum | solution.py:86
  31.3 5.7 %all-reduce.1 = (f32[512]{0:T(512)S(1)}, f32[512]{0:T(512)S(1)}) all-reduce(f32[512]{0:T(512)S(1)} %get-tuple-element.6, f32[512]{0:T(512)S(1)} %get-tuple-element.5), channel_id=1, replica_groups=mesh['sp'=8,'tp'=4] {'tp'}, use_global_device_ids=true, to_apply=%region_3.4 | all-reduce | flops 1024 | bytes 8192 | tf_op jit(solution)/shard_map/psum | solution.py:86
  37.1 0.0 copy-start.1
  37.1 2.1 convolution_convert_fusion.2
  39.3 0.0 reduce-scatter.2.cloned.1.call-update
  39.3 0.0 all-gather.2.cloned.1.call-start
  39.4 0.0 copy-done.4
  39.4 0.1 copy.40
  39.5 0.1 eq.149
  39.6 0.1 eq.145
  39.8 0.6 reduce-window.6
  40.4 0.2 slice_reduce_fusion
  40.6 0.1 copy.39
  40.7 0.1 mul.520
  40.9 0.1 fusion.110
  41.0 1.4 scatter_custom_fusion
  42.4 27.6 %reduce-scatter.2.cloned.1.call-done = bf16[128,2048]{1,0:T(8,128)(2,1)} async-done(((bf16[512,2048]{1,0:T(8,128)(2,1)}), bf16[128,2048]{1,0:T(8,128)(2,1)}) %reduce-scatter.2.cloned.1.call-update) | async-done | bytes 524304 | tf_op jit(solution)/shard_map/reduce_scatter | solution.py:93
  70.0 1.3 fusion.11
  71.3 1.3 fusion.13
  72.7 3.1 gather_fusion
  75.8 42.5 %all_to_all.15 = bf16[8,2,24,2048]{3,2,1,0:T(8,128)(2,1)} all-to-all(bf16[8,2,24,2048]{3,2,1,0:T(8,128)(2,1)} %bitcast.151), channel_id=1, replica_groups=mesh['sp'=8,'tp'=4] {'sp'}, dimensions={0} | all-to-all | bytes 3145728 | tf_op jit(solution)/shard_map/all_to_all | solution.py:124
  118.3 0.0 all-gather.2.cloned.1.call-update
  118.3 44.6 %all-gather.2.cloned.1.call-done = bf16[8,2,96,2048]{3,2,1,0:T(8,128)(2,1)} async-done(((bf16[8,2,24,2048]{3,2,1,0:T(8,128)(2,1)}), bf16[8,2,96,2048]{3,2,1,0:T(8,128)(2,1)}) %all-gather.2.cloned.1.call-update) | async-done | bytes 6291472 | tf_op jit(solution)/shard_map/all_gather | solution.py:125
  162.9 3.6 %fusion.119 = (bf16[8,1,96,2048]{3,2,1,0:T(8,128)(2,1)S(1)}, bf16[8,1,96,2048]{3,2,1,0:T(8,128)(2,1)S(1)}) fusion(bf16[8,2,96,2048]{3,2,1,0:T(8,128)(2,1)} %all-gather.2.cloned.1.call-done), kind=kLoop, calls=%fused_computation.256 | loop fusion | bytes 12582912 | tf_op jit(solution)/shard_map/slice | solution.py:40
  166.4 1.0 fusion.18
  167.4 0.0 copy-start.8
  167.5 1.0 fusion.21
  168.4 0.6 copy-done.8
  169.0 1.0 fusion.10
  170.0 0.0 copy-start.9
  170.0 1.0 fusion.9
  171.0 0.6 copy-done.9
  171.6 1.0 fusion.1
  172.6 1.0 fusion
  173.6 0.6 fusion.5
  174.2 0.8 pad_maximum_fusion
  175.1 74.2 %all_to_all.16 = bf16[4,8,2,1,24,2048]{5,4,1,2,3,0:T(8,128)(2,1)} all-to-all(bf16[4,8,2,1,24,2048]{5,4,1,2,3,0:T(8,128)(2,1)S(1)} %pad_maximum_fusion), channel_id=1, replica_groups=mesh['sp'=8,'tp'=4] {'tp'}, dimensions={0} | all-to-all | bytes 12582912 | tf_op jit(solution)/shard_map/all_to_all | solution.py:128
  249.3 5.7 %reduce_sum.64 = bf16[8,2,24,2048]{3,2,0,1:T(8,128)(2,1)} reduce(bf16[4,8,2,1,24,2048]{5,4,1,2,3,0:T(8,128)(2,1)} %all_to_all.16, bf16[]{:T(256)} %constant.56.clone.1), dimensions={0,3}, to_apply=%region_10.11 | reduce | flops 2359296 | bytes 7864322 | tf_op jit(solution)/shard_map/reduce_sum | solution.py:138
  255.0 2.7 copy.46
  257.7 5.6 %all-to-all-start.2 = ((bf16[8,2,24,2048]{3,2,1,0:T(8,128)(2,1)}), bf16[8,2,24,2048]{3,2,1,0:T(8,128)(2,1)}, u32[]{:S(2)}, u32[]{:S(2)}) async-start(bf16[8,2,24,2048]{3,2,1,0:T(8,128)(2,1)} %copy.46), calls=%async_computation.3 | async-start | bytes 3145728 | tf_op jit(solution)/shard_map/all_to_all | solution.py:139
  263.4 0.1 copy.38
  263.5 36.6 %all-to-all-done.2 = bf16[8,2,24,2048]{3,2,1,0:T(8,128)(2,1)} async-done(((bf16[8,2,24,2048]{3,2,1,0:T(8,128)(2,1)}), bf16[8,2,24,2048]{3,2,1,0:T(8,128)(2,1)}, u32[]{:S(2)}, u32[]{:S(2)}) %all-to-all-start.2) | async-done | bytes 1572896 | tf_op jit(solution)/shard_map/all_to_all | solution.py:139
  300.1 5.0 %gather_fusion.1 = bf16[256,2048]{1,0:T(8,128)(2,1)} fusion(bf16[384,2048]{1,0:T(8,128)(2,1)} %bitcast.59, s32[1024]{0:T(1024)S(1)} %pad_clamp_fusion), kind=kCustom, calls=%fused_computation.1 | custom fusion | bytes 2098176 | tf_op jit(solution)/shard_map/gather | solution.py:141
  305.1 3.4 %reshape.152 = f32[128,2,2048]{2,1,0:T(2,128)} reshape(bf16[256,2048]{1,0:T(8,128)(2,1)} %gather_fusion.1) | data formatting | bytes 3145728 | tf_op jit(solution)/shard_map/convert_element_type | solution.py:141
  308.5 4.9 %multiply_reduce_fusion = f32[128,2048]{1,0:T(8,128)S(1)} fusion(f32[128,2,2048]{2,1,0:T(2,128)} %reshape.152, f32[128,2]{1,0:T(8,128)S(1)} %copy.38), kind=kLoop, calls=%fused_computation.15 | loop fusion | flops 786432 | bytes 3146752 | tf_op jit(solution)/shard_map/reduce_sum | solution.py:142
  313.3 1.0 fusion.14
  (28 shorter events, 0.2 us)
Async XLA Ops:
  6.5 30.6 %copy-start = (bf16[512,2048]{1,0:T(8,128)(2,1)S(1)}, bf16[512,2048]{1,0:T(8,128)(2,1)}, u32[]{:S(2)}) copy-start(bf16[512,2048]{1,0:T(8,128)(2,1)} %param.24) | copy-start | bytes 6291460
  6.5 63.5 %reduce-scatter.2.cloned.1.call-start = ((), (), s32[]{:S(2)}) async-start(), calls=%async_computation.4 | async-start | bytes 2621440 | tf_op jit(solution)/shard_map/reduce_scatter | solution.py:93
  7.4 16.6 %collective-permute-start.2 = (s32[30]{0:T(128)S(1)}, s32[30]{0:T(128)S(1)}, u32[]{:S(2)}, u32[]{:S(2)}) collective-permute-start(s32[30]{0:T(128)S(1)} %slice.325), channel_id=1, source_target_pairs={{0,4},{4,8},{8,12},{12,16},{16,20},{20,24},{24,28},{1,5},{5,9},{9,... | collective-permute-start | bytes 368 | tf_op jit(solution)/shard_map/ppermute | solution.py:13
  13.0 13.4 %collective-permute-start = (bf16[30,128]{1,0:T(8,128)(2,1)S(1)}, bf16[30,128]{1,0:T(8,128)(2,1)S(1)}, u32[]{:S(2)}, u32[]{:S(2)}) collective-permute-start(bf16[30,128]{1,0:T(8,128)(2,1)S(1)} %slice.321), channel_id=1, source_target_pairs={{0,4},{4,8},{8,12},{12,16},{16,20},{20,24},{24,28},{1,5},{5,9},{9,... | collective-permute-start | bytes 23048 | tf_op jit(solution)/shard_map/ppermute | solution.py:13
  17.2 9.2 %collective-permute-start.1 = (bf16[30,128]{1,0:T(8,128)(2,1)S(1)}, bf16[30,128]{1,0:T(8,128)(2,1)S(1)}, u32[]{:S(2)}, u32[]{:S(2)}) collective-permute-start(bf16[30,128]{1,0:T(8,128)(2,1)S(1)} %slice.322), channel_id=1, source_target_pairs={{0,4},{4,8},{8,12},{12,16},{16,20},{20,24},{24,28},{1,5},{5,9},{9,... | collective-permute-start | bytes 23048 | tf_op jit(solution)/shard_map/ppermute | solution.py:13
  37.1 2.2 copy-start.4
  37.1 32.9 %copy-start.1 = (bf16[128,2048]{1,0:T(8,128)(2,1)S(1)}, bf16[128,2048]{1,0:T(8,128)(2,1)}, u32[]{:S(2)}) copy-start(bf16[128,2048]{1,0:T(8,128)(2,1)} %param.16) | copy-start | bytes 1572868
  39.3 32.1 %copy-start.3 = (f32[2048]{0:T(1024)S(1)}, f32[2048]{0:T(1024)}, u32[]{:S(2)}) copy-start(f32[2048]{0:T(1024)} %param.25) | copy-start | bytes 24580
  39.3 123.6 %all-gather.2.cloned.1.call-start = ((), (), s32[]{:S(2)}) async-start(), calls=%async_computation.5 | async-start | bytes 7864320 | tf_op jit(solution)/shard_map/all_gather | solution.py:125
  162.9 3.6 %copy-start.7 = (bf16[2,2048,256]{2,1,0:T(8,128)(2,1)S(1)}, bf16[2,2048,256]{2,1,0:T(8,128)(2,1)}, u32[]{:S(2)}) copy-start(bf16[2,2048,256]{2,1,0:T(8,128)(2,1)} %param.29) | copy-start | bytes 6291460
  167.4 1.6 copy-start.8
  170.0 1.6 copy-start.9
  257.7 5.7 %copy-start.5 = (f32[128,2]{0,1:T(2,128)S(1)}, f32[128,2]{0,1:T(2,128)}, u32[]{:S(2)}) copy-start(f32[128,2]{0,1:T(2,128)} %param.28) | copy-start | bytes 3076
  257.7 5.7 %copy-start.6 = (f32[128]{0:T(128)S(1)}, f32[128]{0:T(128)}, u32[]{:S(2)}) copy-start(f32[128]{0:T(128)} %param.27) | copy-start | bytes 1540
  257.7 42.4 %all-to-all-start.2 = ((bf16[8,2,24,2048]{3,2,1,0:T(8,128)(2,1)}), bf16[8,2,24,2048]{3,2,1,0:T(8,128)(2,1)}, u32[]{:S(2)}, u32[]{:S(2)}) async-start(bf16[8,2,24,2048]{3,2,1,0:T(8,128)(2,1)} %copy.46), calls=%async_computation.3 | async-start | bytes 3145728 | tf_op jit(solution)/shard_map/all_to_all | solution.py:139
  308.5 4.9 %copy-start.2 = (bf16[128,2048]{1,0:T(8,128)(2,1)S(1)}, bf16[128,2048]{1,0:T(8,128)(2,1)}, u32[]{:S(2)}) copy-start(bf16[128,2048]{1,0:T(8,128)(2,1)} %reduce-scatter.2.cloned.1.call-done) | copy-start | bytes 1572868
Sparse Core Ops, SparseCore 0:
  39.4 30.5 reduce-scatter.1
  118.4 44.4 all-gather.1
